TPU v7x, 512 devices: a whole 4x4x16 slice. The times are simulated.
512 devices in a mesh: ep: 128 (over z, x, core), tp: 4 (over y).
Axes of the slice: x: 4, y: 4, z: 16, core: 2. Of those that a mesh axis runs over, the one named last changes fastest.
Arguments:
- tokens: bfloat16 [1024, 2048], P('ep'), may hold values from -6 to 6
- norm_gain: float32 [2048], replicated, may hold values from 0.1 to 1.9
- query_weight: bfloat16 [2048, 1024], P('ep', 'tp'), may hold values from -0.125 to 0.125
- key_weight: bfloat16 [2048, 512], P('ep', 'tp'), may hold values from -0.125 to 0.125
- value_weight: bfloat16 [2048, 512], P('ep', 'tp'), may hold values from -0.125 to 0.125
- query_gain: float32 [64], replicated, may hold values from 0.9 to 1.9
- key_gain: float32 [64], replicated, may hold values from 0.9 to 1.9
- lambdas: float32 [8], P('tp'), may hold values from 0.3 to 0.8
- key_cache: bfloat16 [1024, 4, 320, 128], P('ep', 'tp'), may hold values from -5 to 5
- value_cache: bfloat16 [1024, 4, 320, 128], P('ep', 'tp'), may hold values from -6 to 6
- lengths: int32 [1024], P('ep'), may hold values from 1 to 320
- head_gain: float32 [128], replicated, may hold values from 0.1 to 1.9
- out_weight: bfloat16 [1024, 2048], P('tp', 'ep'), may hold values from -0.1875 to 0.1875
- ffn_gain: float32 [2048], replicated, may hold values from 0.1 to 1.9
- dense_gate_weight: bfloat16 [2048, 1024], P('ep', 'tp'), may hold values from -0.125 to 0.125
- dense_up_weight: bfloat16 [2048, 1024], P('ep', 'tp'), may hold values from -0.125 to 0.125
- dense_down_weight: bfloat16 [1024, 2048], P('tp', 'ep'), may hold values from -0.1875 to 0.1875
- branch_gate: float32 [2048], replicated, may hold values from -0.125 to 0.125
- expert_ids: int32 [1024, 2], P('ep'), may hold values from 0 to 15, all different within a row; in each aligned block of 8 rows (0 to 7, 8 to 15, ...) at most 2 rows name the same one
- expert_probs: float32 [1024, 2], P('ep'), may hold values from 0.1 to 0.9
- expert_gate: bfloat16 [128, 2048, 704], P('ep', None, 'tp'), may hold values from -0.125 to 0.125
- expert_up: bfloat16 [128, 2048, 704], P('ep', None, 'tp'), may hold values from -0.125 to 0.125
- expert_down: bfloat16 [128, 704, 2048], P('ep', 'tp'), may hold values from -0.078125 to 0.078125
Outputs:
- mixed: bfloat16 [1024, 2048], P('ep', 'tp')
Inputs may be any that keep to these rules, and one draw needn't show every extreme that they name: `expert_ids`: each row names 2 different experts. Within each aligned block of 8 rows (the sequences of one index of ep) no expert is named more than 2 times, and in every draw some block names some expert exactly 2 times.
All inputs are finite; a program needn't handle non-finite values.
Results may differ from a plain program's by a relative error of at most 0.014.
Values may be sent and summed in bfloat16 or wider, within the bound.
No kernel may reach another device: no remote copies, remote signals or barrier semaphores. Data moves between devices by JAX's collectives and lax.ppermute only.
A program may use at most 64 MiB of HBM per device.

v0:
```python
import jax
import jax.numpy as jnp
from jax import lax
from jax.sharding import PartitionSpec as P

SUB = 64
VD = 128
EXPERTS = 16
TOP = 2
CAP = 2
epsilon = 1e-06


def rms_scale(values, scaling):
    return values * lax.rsqrt(jnp.mean(values * values, axis=-1, keepdims=True) + epsilon) * scaling


def project_rows(normed, weights):
    stacked = jnp.concatenate(weights, axis=1)
    spread = lax.all_to_all(normed, "ep", split_axis=1, concat_axis=0, tiled=True)
    return lax.psum_scatter(
        jnp.dot(spread, stacked, preferred_element_type=jnp.float32),
        "ep",
        scatter_dimension=0,
        tiled=True,
    )


def project_back(operand, weight):
    products = jnp.dot(
        lax.all_gather(operand, "ep", axis=0, tiled=True),
        weight,
        preferred_element_type=jnp.float32,
    ).astype(jnp.bfloat16)
    partial_value = lax.all_to_all(products, "ep", split_axis=0, concat_axis=1, tiled=True)
    return lax.psum(
        lax.optimization_barrier(partial_value).astype(jnp.float32).astype(jnp.bfloat16), "tp"
    ).astype(jnp.float32)


def attend(packed, key_cache, value_cache, lengths, query_gain, key_gain, lambdas, head_gain):
    seq_here = packed.shape[0]
    kv_here = key_cache.shape[1]
    cache_len = key_cache.shape[2]
    heads_here = lambdas.shape[0]
    per_group = heads_here // kv_here
    query_end = heads_here * 2 * SUB
    key_end = query_end + kv_here * 2 * SUB
    mixed = lax.optimization_barrier(packed.astype(jnp.bfloat16))
    query_parts = rms_scale(
        mixed[:, :query_end].astype(jnp.float32).reshape(seq_here, kv_here, per_group, 2, SUB),
        query_gain,
    ).astype(jnp.bfloat16)
    key_parts = rms_scale(
        mixed[:, query_end:key_end].astype(jnp.float32).reshape(seq_here, kv_here, 2, SUB), key_gain
    ).astype(jnp.bfloat16)
    new_values = mixed[:, key_end:].reshape(seq_here, kv_here, VD)
    cached = rms_scale(
        key_cache.astype(jnp.float32).reshape(seq_here, kv_here, cache_len, 2, SUB), key_gain
    ).astype(jnp.bfloat16)
    score_scale = SUB ** (-0.5)
    scores = (
        jnp.einsum("sgqcd,sgjcd->sgqcj", query_parts, cached, preferred_element_type=jnp.float32)
        * score_scale
    )
    own_score = (
        jnp.einsum("sgqcd,sgcd->sgqc", query_parts, key_parts, preferred_element_type=jnp.float32)
        * score_scale
    )
    live_mask = lax.broadcasted_iota(jnp.int32, (seq_here, cache_len), 1) < lengths[:, None]
    exponent = jnp.where(live_mask[:, None, None, None, :], jnp.exp(scores), 0.0)
    own_exponent = jnp.exp(own_score)
    denominator = jnp.sum(exponent, axis=4) + own_exponent
    shares = exponent / denominator[..., None]
    own_shares = own_exponent / denominator
    lam_heads = lambdas.reshape(1, kv_here, per_group)
    mixing = (shares[:, :, :, 0] - lam_heads[..., None] * shares[:, :, :, 1]).astype(jnp.bfloat16)
    own_mixing = lax.optimization_barrier(
        (own_shares[:, :, :, 0] - lam_heads * own_shares[:, :, :, 1]).astype(jnp.bfloat16)
    )
    head_out = jnp.einsum(
        "sgqj,sgje->sgqe", mixing, value_cache, preferred_element_type=jnp.float32
    )
    head_out = (
        head_out
        + own_mixing.astype(jnp.float32)[..., None] * new_values.astype(jnp.float32)[:, :, None, :]
    )
    return rms_scale(head_out, head_gain).astype(jnp.bfloat16).reshape(seq_here, heads_here * VD)


def route_tables(expert_ids, expert_probs):
    seq_here = expert_ids.shape[0]
    paired = expert_ids.reshape(-1)
    total_pairs = paired.shape[0]
    onehot = (paired[:, None] == lax.broadcasted_iota(jnp.int32, (total_pairs, EXPERTS), 1)).astype(
        jnp.float32
    )
    earlier = (
        lax.broadcasted_iota(jnp.int32, (total_pairs, total_pairs), 1)
        < lax.broadcasted_iota(jnp.int32, (total_pairs, total_pairs), 0)
    ).astype(jnp.float32)
    before = jnp.dot(earlier, onehot, precision=lax.Precision.HIGHEST)
    slot_ranks = jnp.sum(before * onehot, axis=1).astype(jnp.int32)
    slot_codes = (paired * CAP + slot_ranks).reshape(seq_here, TOP)
    slots_iota = lax.broadcasted_iota(jnp.int32, (seq_here, TOP, EXPERTS * CAP), 2)
    picked = (slot_codes[:, :, None] == slots_iota).astype(jnp.float32)
    select = jnp.sum(picked, axis=1)
    combine_weights = jnp.sum(picked * expert_probs[:, :, None], axis=1)
    return (select, combine_weights)


def mixture(ffn_input, expert_ids, expert_probs, expert_gate, expert_up, expert_down):
    here_count = expert_gate.shape[0]
    ep_count = lax.axis_size("ep")
    tp_count = lax.axis_size("tp")
    slot_count = ep_count * here_count
    rep_count = slot_count // EXPERTS
    model_width = ffn_input.shape[1]
    feature_share = model_width // tp_count
    select, combine_weights = route_tables(expert_ids, expert_probs)
    sent_width = ffn_input.shape[1]
    chosen = jnp.einsum(
        "sk,sd->kd", select.astype(jnp.bfloat16), ffn_input, preferred_element_type=jnp.float32
    ).astype(jnp.bfloat16)
    outgoing = jnp.broadcast_to(
        chosen.reshape(1, EXPERTS, CAP, sent_width), (rep_count, EXPERTS, CAP, sent_width)
    ).reshape(slot_count, CAP, sent_width)
    incoming = lax.all_to_all(outgoing, "ep", split_axis=0, concat_axis=0, tiled=True)
    grouped = incoming.reshape(ep_count, here_count, incoming.shape[1], model_width)
    gate_val = jnp.einsum(
        "ihcd,hdf->ihcf", grouped, expert_gate, preferred_element_type=jnp.float32
    )
    up_val = jnp.einsum("ihcd,hdf->ihcf", grouped, expert_up, preferred_element_type=jnp.float32)
    hidden = (jax.nn.silu(gate_val) * up_val).astype(jnp.bfloat16)
    partial_value = jnp.einsum(
        "ihcf,hfd->ihcd", hidden, expert_down, preferred_element_type=jnp.float32
    ).astype(jnp.bfloat16)
    summed = lax.all_to_all(partial_value, "tp", split_axis=3, concat_axis=0, tiled=True)
    block_out = jnp.sum(
        summed.reshape(tp_count, ep_count, here_count, CAP, feature_share).astype(jnp.float32),
        axis=0,
    ).astype(jnp.bfloat16)
    returned = lax.all_to_all(block_out, "ep", split_axis=0, concat_axis=0, tiled=True)
    expert_out = jnp.sum(
        returned.reshape(rep_count, EXPERTS * CAP, feature_share).astype(jnp.float32), axis=0
    )
    return jnp.dot(combine_weights, expert_out, precision=lax.Precision.HIGHEST)


def own_columns(values, tp_start, share_width):
    return lax.dynamic_slice_in_dim(values, tp_start, share_width, 1)


def shards(
    tokens,
    norm_gain,
    query_weight,
    key_weight,
    value_weight,
    query_gain,
    key_gain,
    lambdas,
    key_cache,
    value_cache,
    lengths,
    head_gain,
    out_weight,
    ffn_gain,
    dense_gate_weight,
    dense_up_weight,
    dense_down_weight,
    branch_gate,
    expert_ids,
    expert_probs,
    expert_gate,
    expert_up,
    expert_down,
):
    residual = tokens.astype(jnp.float32)
    normed = rms_scale(residual, norm_gain).astype(jnp.bfloat16)
    packed = project_rows(normed, (query_weight, key_weight, value_weight))
    head_out = attend(
        packed, key_cache, value_cache, lengths, query_gain, key_gain, lambdas, head_gain
    )
    attended = project_back(head_out, out_weight)
    middle = lax.optimization_barrier((residual + attended).astype(jnp.bfloat16))
    middle_f32 = middle.astype(jnp.float32)
    ffn_input = lax.optimization_barrier(rms_scale(middle_f32, ffn_gain).astype(jnp.bfloat16))
    dense_both = project_rows(ffn_input, (dense_gate_weight, dense_up_weight))
    half_width = dense_both.shape[1] // 2
    hidden = (jax.nn.silu(dense_both[:, :half_width]) * dense_both[:, half_width:]).astype(
        jnp.bfloat16
    )
    dense = project_back(hidden, dense_down_weight)
    branch_weight = jax.nn.sigmoid(
        jnp.sum(ffn_input.astype(jnp.float32) * branch_gate, axis=1, keepdims=True)
    )
    routed = mixture(ffn_input, expert_ids, expert_probs, expert_gate, expert_up, expert_down)
    share_width = routed.shape[1]
    tp_start = lax.axis_index("tp") * share_width
    combined = (
        own_columns(middle_f32, tp_start, share_width)
        + own_columns(branch_weight * dense, tp_start, share_width)
        + routed
    )
    return combined.astype(jnp.bfloat16)


def solution(mesh):
    return jax.shard_map(
        shards,
        mesh=mesh,
        in_specs=(
            P("ep", None),
            P(),
            P("ep", "tp"),
            P("ep", "tp"),
            P("ep", "tp"),
            P(),
            P(),
            P("tp"),
            P("ep", "tp", None, None),
            P("ep", "tp", None, None),
            P("ep"),
            P(),
            P("tp", "ep"),
            P(),
            P("ep", "tp"),
            P("ep", "tp"),
            P("tp", "ep"),
            P(),
            P("ep", None),
            P("ep", None),
            P("ep", None, "tp"),
            P("ep", None, "tp"),
            P("ep", "tp", None),
        ),
        out_specs=P("ep", "tp"),
        check_vma=False,
    )
```

profile of v0, /device:TPU:33, one launch (start us, length us, event | category | flops | bytes accessed | tf_op | source)
XLA Modules:
  0.0 908.0 jit_solution(11844619829971463060)
XLA Ops:
  6.5 1.0 fusion.32
  7.5 0.8 fusion.34
  8.8 41.7 %all_to_all.98 = bf16[8,128,16]{2,0,1:T(8,128)(2,1)S(1)} all-to-all(bf16[8,128,16]{2,0,1:T(8,128)(2,1)S(1)} %copy.97), channel_id=1, replica_groups=mesh['ep'=128,'tp'=4] {'ep'}, dimensions={1} | all-to-all | bytes 65536 | tf_op jit(solution)/shard_map/all_to_all | solution.py:20
  50.4 2.5 fusion.24
  52.9 1.1 copy-done.2
  55.5 239.6 %reduce-scatter.3.cloned.1.call-done = f32[8,512]{1,0:T(8,128)} async-done(((f32[1024,512]{1,0:T(8,128)}), f32[8,512]{1,0:T(8,128)}) %reduce-scatter.3.cloned.1.call-update) | async-done | bytes 16400 | tf_op jit(solution)/shard_map/reduce_scatter | solution.py:21
  298.4 93.9 %all_gather.6 = bf16[1024,256]{1,0:T(8,128)(2,1)S(1)} all-gather(bf16[8,256]{1,0:T(8,128)(2,1)S(1)} %bitcast.148), channel_id=1, replica_groups=mesh['ep'=128,'tp'=4] {'ep'}, dimensions={0}, use_global_device_ids=true | all-gather | bytes 528384 | tf_op jit(solution)/shard_map/all_gather | solution.py:31
  392.6 0.9 copy.106
  393.4 12.8 %all-to-all-start.1 = ((bf16[128,8,16]{2,1,0:T(8,128)(2,1)}), bf16[128,8,16]{2,1,0:T(8,128)(2,1)S(1)}, u32[]{:S(2)}, u32[]{:S(2)}) async-start(bf16[128,8,16]{2,1,0:T(8,128)(2,1)} %bitcast.18), calls=%async_computation.2 | async-start | bytes 524288 | tf_op jit(solution)/shard_map/all_to_all | solution.py:35
  406.4 22.4 %all-to-all-done.1 = bf16[128,8,16]{2,1,0:T(8,128)(2,1)S(1)} async-done(((bf16[128,8,16]{2,1,0:T(8,128)(2,1)}), bf16[128,8,16]{2,1,0:T(8,128)(2,1)S(1)}, u32[]{:S(2)}, u32[]{:S(2)}) %all-to-all-start.1) | async-done | bytes 32800 | tf_op jit(solution)/shard_map/all_to_all | solution.py:35
  429.2 13.3 %psum.14 = bf16[8,2048]{1,0:T(8,128)(2,1)S(1)} all-reduce(bf16[8,2048]{1,0:T(8,128)(2,1)S(1)} %all_to_all.78), channel_id=1, replica_groups=mesh['ep'=128,'tp'=4] {'tp'}, use_global_device_ids=true, to_apply=%region_7.8 | all-reduce | flops 16384 | bytes 65536 | tf_op jit(solution)/shard_map/psum | solution.py:36
  443.4 0.9 copy.108
  444.3 9.9 %all-to-all-start.2 = ((bf16[8,128,16]{2,0,1:T(8,128)(2,1)}), bf16[8,128,16]{2,0,1:T(8,128)(2,1)S(1)}, u32[]{:S(2)}, u32[]{:S(2)}) async-start(bf16[8,128,16]{2,0,1:T(8,128)(2,1)} %copy.108), calls=%async_computation.3 | async-start | bytes 524288 | tf_op jit(solution)/shard_map/all_to_all | solution.py:20
  454.6 22.2 %all-to-all-done.2 = bf16[8,128,16]{2,0,1:T(8,128)(2,1)S(1)} async-done(((bf16[8,128,16]{2,0,1:T(8,128)(2,1)}), bf16[8,128,16]{2,0,1:T(8,128)(2,1)S(1)}, u32[]{:S(2)}, u32[]{:S(2)}) %all-to-all-start.2) | async-done | bytes 32800 | tf_op jit(solution)/shard_map/all_to_all | solution.py:20
  476.8 1.7 broadcast_in_dim.19
  478.5 6.2 all-to-all-start.4
  484.8 1.7 fusion.22
  486.5 53.7 %all-to-all-done.4 = bf16[128,2,2048]{2,1,0:T(2,128)(2,1)S(1)} async-done(((bf16[128,2,2048]{2,1,0:T(2,128)(2,1)}), bf16[128,2,2048]{2,1,0:T(2,128)(2,1)S(1)}, u32[]{:S(2)}, u32[]{:S(2)}) %all-to-all-start.4) | async-done | bytes 1048608 | tf_op jit(solution)/shard_map/all_to_all | solution.py:128
  540.3 1.5 convolution_bitcast_fusion.1
  541.8 2.4 fusion
  544.1 2.0 copy.116
  546.2 3.6 all-to-all-start.5
  549.8 190.6 %reduce-scatter.5.cloned.1.call-done = f32[8,512]{1,0:T(8,128)} async-done(((f32[1024,512]{1,0:T(8,128)}), f32[8,512]{1,0:T(8,128)}) %reduce-scatter.5.cloned.1.call-update) | async-done | bytes 16400 | tf_op jit(solution)/shard_map/reduce_scatter | solution.py:21
  741.2 93.9 %all_gather.7 = bf16[1024,256]{1,0:T(8,128)(2,1)S(1)} all-gather(bf16[8,256]{1,0:T(8,128)(2,1)S(1)} %fusion.50), channel_id=1, replica_groups=mesh['ep'=128,'tp'=4] {'ep'}, dimensions={0}, use_global_device_ids=true | all-gather | bytes 528384 | tf_op jit(solution)/shard_map/all_gather | solution.py:31
  835.3 0.9 copy.109
  836.1 12.8 %all-to-all-start.3 = ((bf16[128,8,16]{2,1,0:T(8,128)(2,1)}), bf16[128,8,16]{2,1,0:T(8,128)(2,1)S(1)}, u32[]{:S(2)}, u32[]{:S(2)}) async-start(bf16[128,8,16]{2,1,0:T(8,128)(2,1)} %bitcast.22), calls=%async_computation.5 | async-start | bytes 524288 | tf_op jit(solution)/shard_map/all_to_all | solution.py:35
  849.0 1.6 reduce_sum.136
  850.7 1.0 copy.118
  851.7 19.8 %all-to-all-done.3 = bf16[128,8,16]{2,1,0:T(8,128)(2,1)S(1)} async-done(((bf16[128,8,16]{2,1,0:T(8,128)(2,1)}), bf16[128,8,16]{2,1,0:T(8,128)(2,1)S(1)}, u32[]{:S(2)}, u32[]{:S(2)}) %all-to-all-start.3) | async-done | bytes 32800 | tf_op jit(solution)/shard_map/all_to_all | solution.py:35
  871.5 6.2 all-to-all-start.6
  878.3 14.5 %psum.15 = bf16[8,2048]{1,0:T(8,128)(2,1)S(1)} all-reduce(bf16[8,2048]{1,0:T(8,128)(2,1)S(1)} %all_to_all.86), channel_id=1, replica_groups=mesh['ep'=128,'tp'=4] {'tp'}, use_global_device_ids=true, to_apply=%region_11.12 | all-reduce | flops 16384 | bytes 65536 | tf_op jit(solution)/shard_map/psum | solution.py:36
  892.8 7.5 all-to-all-done.6
  (120 shorter events, 9.7 us)
Async XLA Ops:
  6.5 535.2 %copy-start = (bf16[1,176,2048]{2,1,0:T(8,128)(2,1)S(1)}, bf16[1,176,2048]{2,1,0:T(8,128)(2,1)}, u32[]{:S(2)}) copy-start(bf16[1,176,2048]{2,1,0:T(8,128)(2,1)} %param.45) | copy-start | bytes 2162692
  6.5 288.6 %reduce-scatter.3.cloned.1.call-start = ((), (), s32[]{:S(2)}) async-start(), calls=%async_computation.9 | async-start | bytes 2113536 | tf_op jit(solution)/shard_map/reduce_scatter | solution.py:21
  52.9 1.1 copy-start.2
  52.9 1.5 copy-start.14
  54.8 0.7 copy-start.17
  54.8 241.8 %copy-start.18 = (f32[64]{0:T(128)S(1)}, f32[64]{0:T(128)}, u32[]{:S(2)}) copy-start(f32[64]{0:T(128)} %param.29) | copy-start | bytes 772
  54.8 241.9 %copy-start.16 = (f32[64]{0:T(128)S(1)}, f32[64]{0:T(128)}, u32[]{:S(2)}) copy-start(f32[64]{0:T(128)} %param.28) | copy-start | bytes 772
  54.9 242.7 %copy-start.20 = (f32[2]{0:T(128)S(1)}, f32[2]{0:T(128)}, u32[]{:S(2)}) copy-start(f32[2]{0:T(128)} %param.30) | copy-start | bytes 28
  55.4 242.5 %copy-start.22 = (bf16[8,1,320,128]{3,2,1,0:T(8,128)(2,1)S(1)}, bf16[8,1,320,128]{3,2,1,0:T(8,128)(2,1)}, u32[]{:S(2)}) copy-start(bf16[8,1,320,128]{3,2,1,0:T(8,128)(2,1)} %param.32) | copy-start | bytes 1966084
  55.4 242.9 %copy-start.19 = (f32[128]{0:T(128)S(1)}, f32[128]{0:T(128)}, u32[]{:S(2)}) copy-start(f32[128]{0:T(128)} %param.34) | copy-start | bytes 1540
  297.0 95.3 %copy-start.8 = (bf16[256,16]{0,1:T(8,128)(2,1)S(1)}, bf16[256,16]{0,1:T(8,128)(2,1)}, u32[]{:S(2)}) copy-start(bf16[256,16]{0,1:T(8,128)(2,1)} %param.35) | copy-start | bytes 24580
  297.5 108.9 %copy-start.15 = (f32[8,2]{0,1:T(2,128)S(1)}, f32[8,2]{0,1:T(2,128)}, u32[]{:S(2)}) copy-start(f32[8,2]{0,1:T(2,128)} %param.42) | copy-start | bytes 196
  298.3 144.2 %copy-start.7 = (bf16[8,2048]{1,0:T(8,128)(2,1)S(1)}, bf16[8,2048]{1,0:T(8,128)(2,1)}, u32[]{:S(2)}) copy-start(bf16[8,2048]{1,0:T(8,128)(2,1)} %param.23) | copy-start | bytes 98308
  298.3 144.8 %copy-start.12 = (f32[2048]{0:T(1024)S(1)}, f32[2048]{0:T(1024)}, u32[]{:S(2)}) copy-start(f32[2048]{0:T(1024)} %param.36) | copy-start | bytes 24580
  393.4 35.4 %all-to-all-start.1 = ((bf16[128,8,16]{2,1,0:T(8,128)(2,1)}), bf16[128,8,16]{2,1,0:T(8,128)(2,1)S(1)}, u32[]{:S(2)}, u32[]{:S(2)}) async-start(bf16[128,8,16]{2,1,0:T(8,128)(2,1)} %bitcast.18), calls=%async_computation.2 | async-start | bytes 524288 | tf_op jit(solution)/shard_map/all_to_all | solution.py:35
  442.5 0.6 copy-start.3
  443.2 35.3 %copy-start.5 = (bf16[8,2048]{1,0:T(8,128)(2,1)}, bf16[8,2048]{1,0:T(8,128)(2,1)S(1)}, u32[]{:S(2)}) copy-start(bf16[8,2048]{1,0:T(8,128)(2,1)S(1)} %multiply_convert_fusion.2) | copy-start | bytes 98308
  444.3 32.5 %all-to-all-start.2 = ((bf16[8,128,16]{2,0,1:T(8,128)(2,1)}), bf16[8,128,16]{2,0,1:T(8,128)(2,1)S(1)}, u32[]{:S(2)}, u32[]{:S(2)}) async-start(bf16[8,128,16]{2,0,1:T(8,128)(2,1)} %copy.108), calls=%async_computation.3 | async-start | bytes 524288 | tf_op jit(solution)/shard_map/all_to_all | solution.py:20
  454.6 30.2 %copy-start.9 = (bf16[16,256]{1,0:T(8,128)(2,1)S(1)}, bf16[16,256]{1,0:T(8,128)(2,1)}, u32[]{:S(2)}) copy-start(bf16[16,256]{1,0:T(8,128)(2,1)} %param.38) | copy-start | bytes 24580
  454.6 30.2 %copy-start.10 = (bf16[16,256]{1,0:T(8,128)(2,1)S(1)}, bf16[16,256]{1,0:T(8,128)(2,1)}, u32[]{:S(2)}) copy-start(bf16[16,256]{1,0:T(8,128)(2,1)} %param.37) | copy-start | bytes 24580
  478.5 61.8 %all-to-all-start.4 = ((bf16[128,2,2048]{2,1,0:T(2,128)(2,1)}), bf16[128,2,2048]{2,1,0:T(2,128)(2,1)S(1)}, u32[]{:S(2)}, u32[]{:S(2)}) async-start(bf16[128,2,2048]{2,1,0:T(2,128)(2,1)} %bitcast.24), calls=%async_computation.6 | async-start | bytes 2097152 | tf_op jit(solution)/shard_map/all_to_all | solution.py:128
  484.7 255.7 %reduce-scatter.5.cloned.1.call-start = ((), (), s32[]{:S(2)}) async-start(), calls=%async_computation.10 | async-start | bytes 2113536 | tf_op jit(solution)/shard_map/reduce_scatter | solution.py:21
  486.5 53.8 %copy-start.21 = (bf16[1,2048,176]{1,2,0:T(8,128)(2,1)S(1)}, bf16[1,2048,176]{1,2,0:T(8,128)(2,1)}, u32[]{:S(2)}) copy-start(bf16[1,2048,176]{1,2,0:T(8,128)(2,1)} %param.43) | copy-start | bytes 2162692
  486.5 55.2 %copy-start.1 = (bf16[1,2048,176]{1,2,0:T(8,128)(2,1)S(1)}, bf16[1,2048,176]{1,2,0:T(8,128)(2,1)}, u32[]{:S(2)}) copy-start(bf16[1,2048,176]{1,2,0:T(8,128)(2,1)} %param.44) | copy-start | bytes 2162692
  546.2 288.9 %copy-start.11 = (bf16[256,16]{0,1:T(8,128)(2,1)S(1)}, bf16[256,16]{0,1:T(8,128)(2,1)}, u32[]{:S(2)}) copy-start(bf16[256,16]{0,1:T(8,128)(2,1)} %param.39) | copy-start | bytes 24580
  546.2 290.0 %all-to-all-start.5 = ((bf16[128,1,2,2048]{0,2,1,3:T(2,128)(2,1)}), bf16[128,1,2,2048]{0,2,1,3:T(2,128)(2,1)S(1)}, u32[]{:S(2)}, u32[]{:S(2)}) async-start(bf16[128,1,2,2048]{0,2,1,3:T(2,128)(2,1)} %copy.116), calls=%async_computation.7 | async-start | bytes 2097152 | tf_op jit(solution)/shard_map/all_to_all | solution.py:138
  836.1 35.4 %all-to-all-start.3 = ((bf16[128,8,16]{2,1,0:T(8,128)(2,1)}), bf16[128,8,16]{2,1,0:T(8,128)(2,1)S(1)}, u32[]{:S(2)}, u32[]{:S(2)}) async-start(bf16[128,8,16]{2,1,0:T(8,128)(2,1)} %bitcast.22), calls=%async_computation.5 | async-start | bytes 524288 | tf_op jit(solution)/shard_map/all_to_all | solution.py:35
  849.0 28.8 %copy-start.4 = (bf16[8,2048]{1,0:T(8,128)(2,1)S(1)}, bf16[8,2048]{1,0:T(8,128)(2,1)}, u32[]{:S(2)}) copy-start(bf16[8,2048]{1,0:T(8,128)(2,1)} %copy-done.3) | copy-start | bytes 98308
  849.0 28.8 %copy-start.6 = (bf16[8,2048]{1,0:T(8,128)(2,1)S(1)}, bf16[8,2048]{1,0:T(8,128)(2,1)}, u32[]{:S(2)}) copy-start(bf16[8,2048]{1,0:T(8,128)(2,1)} %copy-done.5) | copy-start | bytes 98308
  849.0 28.8 %copy-start.13 = (f32[2048]{0:T(1024)S(1)}, f32[2048]{0:T(1024)}, u32[]{:S(2)}) copy-start(f32[2048]{0:T(1024)} %param.40) | copy-start | bytes 24580
  871.5 28.8 %all-to-all-start.6 = ((bf16[128,1,2,512]{3,2,1,0:T(2,128)(2,1)}), bf16[128,1,2,512]{3,2,1,0:T(2,128)(2,1)S(1)}, u32[]{:S(2)}, u32[]{:S(2)}) async-start(bf16[128,1,2,512]{3,2,1,0:T(2,128)(2,1)} %copy.118), calls=%async_computation.8 | async-start | bytes 524288 | tf_op jit(solution)/shard_map/all_to_all | solution.py:143
Sparse Core Ops, SparseCore 0:
  53.0 242.0 reduce-scatter.2
  490.1 250.2 reduce-scatter.4
where the time goes:
time: 909 us; the launch traced here: 908 us
  waiting for transfers between devices  556 us (61%)
  blocking collectives  257 us (28%)
  starting transfers between devices  51.6 us (6%)
  between operations  13.8 us (2%)
  local copies, waits for them, and re-layouts  12.5 us (1%)
  matrix products  10.6 us (1%)
    reduce_scatter x2, waiting for transfers between devices, project_rows(): lax.psum_scatter(jnp.dot(spread, stacked, preferred_element_type=jnp.floa...  430 us
    all_gather x2, blocking collectives, project_back(): lax.all_gather(operand, 'ep', axis=0, tiled=True)  188 us
    all_to_all x1, waiting for transfers between devices, mixture(): lax.all_to_all(outgoing, 'ep', split_axis=0, concat_axis=0, tiled=True)  53.7 us
    all_to_all x2, waiting for transfers between devices, project_back(): lax.all_to_all(products, 'ep', split_axis=0, concat_axis=1, tiled=True)  42.2 us
    all_to_all x1, blocking collectives, project_rows(): lax.all_to_all(normed, 'ep', split_axis=1, concat_axis=0, tiled=True)  41.7 us
    psum x2, blocking collectives, project_back(): lax.psum(lax.optimization_barrier(partial_value).astype(jnp.float32).asty...  27.8 us
    all_to_all x2, starting transfers between devices, project_back(): lax.all_to_all(products, 'ep', split_axis=0, concat_axis=1, tiled=True)  25.6 us
    all_to_all x1, waiting for transfers between devices, project_rows(): lax.all_to_all(normed, 'ep', split_axis=1, concat_axis=0, tiled=True)  22.2 us
  transfers between devices with their start and end apart: 8, of which 7 were waited for; matrix products, arithmetic and copies ran while one was open for 2% of the time, Pallas kernels for 0%

commit v1 on v0

--- a/solution.py
+++ b/solution.py
@@ -9,6 +9,11 @@
 TOP = 2
 CAP = 2
 epsilon = 1e-06
+
+
+def gather_over(value, name, dim):
+    sent = jnp.stack([value] * lax.axis_size(name))
+    return jnp.concatenate(lax.all_to_all(sent, name, 0, 0), axis=dim)
 
 
 def rms_scale(values, scaling):
@@ -28,9 +33,7 @@
 
 def project_back(operand, weight):
     products = jnp.dot(
-        lax.all_gather(operand, "ep", axis=0, tiled=True),
-        weight,
-        preferred_element_type=jnp.float32,
+        gather_over(operand, "ep", 0), weight, preferred_element_type=jnp.float32
     ).astype(jnp.bfloat16)
     partial_value = lax.all_to_all(products, "ep", split_axis=0, concat_axis=1, tiled=True)
     return lax.psum(

time: 909 us -> 845 us (0.930)
  blocking collectives: 257 us -> 67.8 us
  waiting for transfers between devices: 556 us -> 642 us
  starting transfers between devices: 51.6 us -> 89.4 us
    all_gather x2 -> x0, blocking collectives: 188 us -> none  [project_back(): lax.all_gather(operand, 'ep', axis=0, tiled=True)]
    reduce_scatter x2, waiting for transfers between devices: 430 us -> 494 us  [project_rows(): lax.psum_scatter(jnp.dot(spread, stacked, preferred_element_type=jnp.floa...]
    all_to_all x0 -> x2, waiting for transfers between devices: none -> 60.9 us  [gather_over(): return jnp.concatenate(lax.all_to_all(sent, name, 0, 0), axis=dim)]
    all_to_all x1, waiting for transfers between devices: 53.7 us -> 0.01 us  [mixture(): lax.all_to_all(outgoing, 'ep', split_axis=0, concat_axis=0, tiled=True)]
    all_to_all x0 -> x2, starting transfers between devices: none -> 50.4 us  [gather_over(): return jnp.concatenate(lax.all_to_all(sent, name, 0, 0), axis=dim)]
    all_to_all x1, waiting for transfers between devices: 0.01 us -> 14 us  [mixture(): lax.all_to_all(partial_value, 'tp', split_axis=3, concat_axis=0, tiled=True)]
    all_to_all x2, starting transfers between devices: 25.6 us -> 12.6 us  [project_back(): lax.all_to_all(products, 'ep', split_axis=0, concat_axis=1, tiled=True)]
  transfers between devices with their start and end apart: 8 -> 10, of which waited for: 7 -> 9; matrix products, arithmetic and copies ran while one was open for 2% -> 2% of each run, Pallas kernels for 0% -> 0%
where the time goes in v1:
time: 845 us; the launch traced here: 844 us
  waiting for transfers between devices  642 us (76%)
  starting transfers between devices  89.4 us (11%)
  blocking collectives  67.8 us (8%)
  between operations  13.8 us (2%)
  local copies, waits for them, and re-layouts  13.7 us (2%)
  matrix products  10.8 us (1%)
    reduce_scatter x2, waiting for transfers between devices, project_rows(): lax.psum_scatter(jnp.dot(spread, stacked, preferred_element_type=jnp.floa...  494 us
    all_to_all x2, waiting for transfers between devices, gather_over(): return jnp.concatenate(lax.all_to_all(sent, name, 0, 0), axis=dim)  60.9 us
    all_to_all x2, starting transfers between devices, gather_over(): return jnp.concatenate(lax.all_to_all(sent, name, 0, 0), axis=dim)  50.4 us
    all_to_all x2, waiting for transfers between devices, project_back(): lax.all_to_all(products, 'ep', split_axis=0, concat_axis=1, tiled=True)  42.4 us
    all_to_all x1, blocking collectives, project_rows(): lax.all_to_all(normed, 'ep', split_axis=1, concat_axis=0, tiled=True)  41.7 us
    psum x2, blocking collectives, project_back(): lax.psum(lax.optimization_barrier(partial_value).astype(jnp.float32).asty...  26.2 us
    all_to_all x1, waiting for transfers between devices, project_rows(): lax.all_to_all(normed, 'ep', split_axis=1, concat_axis=0, tiled=True)  22.2 us
  transfers between devices with their start and end apart: 10, of which 9 were waited for; matrix products, arithmetic and copies ran while one was open for 2% of the time, Pallas kernels for 0%

profile of v1, /device:TPU:33, one launch (start us, length us, event | category | flops | bytes accessed | tf_op | source)
XLA Modules:
  0.0 844.3 jit_solution(6923498952099144837)
XLA Ops:
  6.5 1.0 fusion.34
  8.8 41.7 %all_to_all.108 = bf16[8,128,16]{2,0,1:T(8,128)(2,1)S(1)} all-to-all(bf16[8,128,16]{2,0,1:T(8,128)(2,1)S(1)} %copy.97), channel_id=1, replica_groups=mesh['ep'=128,'tp'=4] {'ep'}, dimensions={1} | all-to-all | bytes 65536 | tf_op jit(solution)/shard_map/all_to_all | solution.py:25
  50.4 2.5 fusion.26
  52.9 1.1 copy-done.1
  55.1 240.0 %reduce-scatter.3.cloned.1.call-done = f32[8,512]{1,0:T(8,128)} async-done(((f32[1024,512]{1,0:T(8,128)}), f32[8,512]{1,0:T(8,128)}) %reduce-scatter.3.cloned.1.call-update) | async-done | bytes 16400 | tf_op jit(solution)/shard_map/reduce_scatter | solution.py:26
  299.2 25.3 %all-to-all-start.1 = ((bf16[128,8,256]{2,1,0:T(8,128)(2,1)}), bf16[128,8,256]{2,1,0:T(8,128)(2,1)S(1)}, u32[]{:S(2)}, u32[]{:S(2)}) async-start(bf16[128,8,256]{2,1,0:T(8,128)(2,1)} %stack.4), calls=%async_computation.2 | async-start | bytes 1048576 | tf_op jit(solution)/shard_map/all_to_all | solution.py:16
  324.9 33.3 %all-to-all-done.1 = bf16[128,8,256]{2,1,0:T(8,128)(2,1)S(1)} async-done(((bf16[128,8,256]{2,1,0:T(8,128)(2,1)}), bf16[128,8,256]{2,1,0:T(8,128)(2,1)S(1)}, u32[]{:S(2)}, u32[]{:S(2)}) %all-to-all-start.1) | async-done | bytes 524320 | tf_op jit(solution)/shard_map/all_to_all | solution.py:16
  359.3 6.2 all-to-all-start.2
  365.7 22.4 %all-to-all-done.2 = bf16[128,8,16]{2,1,0:T(8,128)(2,1)S(1)} async-done(((bf16[128,8,16]{2,1,0:T(8,128)(2,1)}), bf16[128,8,16]{2,1,0:T(8,128)(2,1)S(1)}, u32[]{:S(2)}, u32[]{:S(2)}) %all-to-all-start.2) | async-done | bytes 32800 | tf_op jit(solution)/shard_map/all_to_all | solution.py:38
  388.5 13.3 %psum.14 = bf16[8,2048]{1,0:T(8,128)(2,1)S(1)} all-reduce(bf16[8,2048]{1,0:T(8,128)(2,1)S(1)} %all_to_all.85), channel_id=1, replica_groups=mesh['ep'=128,'tp'=4] {'tp'}, use_global_device_ids=true, to_apply=%region_7.8 | all-reduce | flops 16384 | bytes 65536 | tf_op jit(solution)/shard_map/psum | solution.py:39
  402.3 0.9 copy.108
  403.1 9.9 %all-to-all-start.3 = ((bf16[8,128,16]{2,0,1:T(8,128)(2,1)}), bf16[8,128,16]{2,0,1:T(8,128)(2,1)S(1)}, u32[]{:S(2)}, u32[]{:S(2)}) async-start(bf16[8,128,16]{2,0,1:T(8,128)(2,1)} %copy.108), calls=%async_computation.4 | async-start | bytes 524288 | tf_op jit(solution)/shard_map/all_to_all | solution.py:25
  413.4 22.2 %all-to-all-done.3 = bf16[8,128,16]{2,0,1:T(8,128)(2,1)S(1)} async-done(((bf16[8,128,16]{2,0,1:T(8,128)(2,1)}), bf16[8,128,16]{2,0,1:T(8,128)(2,1)S(1)}, u32[]{:S(2)}, u32[]{:S(2)}) %all-to-all-start.3) | async-done | bytes 32800 | tf_op jit(solution)/shard_map/all_to_all | solution.py:25
  435.6 1.7 broadcast_in_dim.19
  437.3 6.2 all-to-all-start.6
  443.6 1.7 fusion.24
  445.4 253.9 %reduce-scatter.5.cloned.1.call-done = f32[8,512]{1,0:T(8,128)} async-done(((f32[1024,512]{1,0:T(8,128)}), f32[8,512]{1,0:T(8,128)}) %reduce-scatter.5.cloned.1.call-update) | async-done | bytes 16400 | tf_op jit(solution)/shard_map/reduce_scatter | solution.py:26
  700.9 25.1 %all-to-all-start.4 = ((bf16[128,8,256]{2,1,0:T(8,128)(2,1)}), bf16[128,8,256]{2,1,0:T(8,128)(2,1)S(1)}, u32[]{:S(2)}, u32[]{:S(2)}) async-start(bf16[128,8,256]{2,1,0:T(8,128)(2,1)} %stack.5), calls=%async_computation.6 | async-start | bytes 1048576 | tf_op jit(solution)/shard_map/all_to_all | solution.py:16
  726.0 1.5 convolution_bitcast_fusion.1
  727.5 2.6 fusion
  730.1 2.0 copy.116
  732.1 27.6 %all-to-all-done.4 = bf16[128,8,256]{2,1,0:T(8,128)(2,1)S(1)} async-done(((bf16[128,8,256]{2,1,0:T(8,128)(2,1)}), bf16[128,8,256]{2,1,0:T(8,128)(2,1)S(1)}, u32[]{:S(2)}, u32[]{:S(2)}) %all-to-all-start.4) | async-done | bytes 524320 | tf_op jit(solution)/shard_map/all_to_all | solution.py:16
  759.7 4.0 all-to-all-start.7
  764.0 0.9 copy.109
  764.9 14.0 %all-to-all-done.7 = bf16[128,1,2,2048]{0,2,1,3:T(2,128)(2,1)S(1)} async-done(((bf16[128,1,2,2048]{0,2,1,3:T(2,128)(2,1)}), bf16[128,1,2,2048]{0,2,1,3:T(2,128)(2,1)S(1)}, u32[]{:S(2)}, u32[]{:S(2)}) %all-to-all-start.7) | async-done | bytes 1048608 | tf_op jit(solution)/shard_map/all_to_all | solution.py:141
  778.8 6.4 all-to-all-start.5
  785.2 1.5 reduce_sum.136
  786.8 1.0 copy.118
  787.8 20.0 %all-to-all-done.5 = bf16[128,8,16]{2,1,0:T(8,128)(2,1)S(1)} async-done(((bf16[128,8,16]{2,1,0:T(8,128)(2,1)}), bf16[128,8,16]{2,1,0:T(8,128)(2,1)S(1)}, u32[]{:S(2)}, u32[]{:S(2)}) %all-to-all-start.5) | async-done | bytes 32800 | tf_op jit(solution)/shard_map/all_to_all | solution.py:38
  807.8 6.2 all-to-all-start.8
  814.5 12.9 %psum.15 = bf16[8,2048]{1,0:T(8,128)(2,1)S(1)} all-reduce(bf16[8,2048]{1,0:T(8,128)(2,1)S(1)} %all_to_all.94), channel_id=1, replica_groups=mesh['ep'=128,'tp'=4] {'tp'}, use_global_device_ids=true, to_apply=%region_11.12 | all-reduce | flops 16384 | bytes 65536 | tf_op jit(solution)/shard_map/psum | solution.py:39
  827.4 9.1 %all-to-all-done.8 = bf16[128,1,2,512]{3,2,1,0:T(2,128)(2,1)S(1)} async-done(((bf16[128,1,2,512]{3,2,1,0:T(2,128)(2,1)}), bf16[128,1,2,512]{3,2,1,0:T(2,128)(2,1)S(1)}, u32[]{:S(2)}, u32[]{:S(2)}) %all-to-all-start.8) | async-done | bytes 262176 | tf_op jit(solution)/shard_map/all_to_all | solution.py:146
  (114 shorter events, 12.6 us)
Async XLA Ops:
  6.5 721.0 %copy-start = (bf16[1,176,2048]{2,1,0:T(8,128)(2,1)S(1)}, bf16[1,176,2048]{2,1,0:T(8,128)(2,1)}, u32[]{:S(2)}) copy-start(bf16[1,176,2048]{2,1,0:T(8,128)(2,1)} %param.45) | copy-start | bytes 2162692
  6.5 288.6 %reduce-scatter.3.cloned.1.call-start = ((), (), s32[]{:S(2)}) async-start(), calls=%async_computation.11 | async-start | bytes 2113536 | tf_op jit(solution)/shard_map/reduce_scatter | solution.py:26
  52.9 1.1 copy-start.1
  54.3 0.7 copy-start.12
  54.4 242.2 %copy-start.13 = (f32[64]{0:T(128)S(1)}, f32[64]{0:T(128)}, u32[]{:S(2)}) copy-start(f32[64]{0:T(128)} %param.29) | copy-start | bytes 772
  54.4 242.3 %copy-start.11 = (f32[64]{0:T(128)S(1)}, f32[64]{0:T(128)}, u32[]{:S(2)}) copy-start(f32[64]{0:T(128)} %param.28) | copy-start | bytes 772
  54.5 243.1 %copy-start.15 = (f32[2]{0:T(128)S(1)}, f32[2]{0:T(128)}, u32[]{:S(2)}) copy-start(f32[2]{0:T(128)} %param.30) | copy-start | bytes 28
  55.0 242.9 %copy-start.17 = (bf16[8,1,320,128]{3,2,1,0:T(8,128)(2,1)S(1)}, bf16[8,1,320,128]{3,2,1,0:T(8,128)(2,1)}, u32[]{:S(2)}) copy-start(bf16[8,1,320,128]{3,2,1,0:T(8,128)(2,1)} %param.32) | copy-start | bytes 1966084
  55.0 243.3 %copy-start.14 = (f32[128]{0:T(128)S(1)}, f32[128]{0:T(128)}, u32[]{:S(2)}) copy-start(f32[128]{0:T(128)} %param.34) | copy-start | bytes 1540
  297.4 27.1 %copy-start.9 = (s32[8,2]{0,1:T(2,128)S(1)}, s32[8,2]{0,1:T(2,128)}, u32[]{:S(2)}) copy-start(s32[8,2]{0,1:T(2,128)} %param.41) | copy-start | bytes 196
  297.4 60.8 %copy-start.3 = (bf16[256,16]{0,1:T(8,128)(2,1)S(1)}, bf16[256,16]{0,1:T(8,128)(2,1)}, u32[]{:S(2)}) copy-start(bf16[256,16]{0,1:T(8,128)(2,1)} %param.35) | copy-start | bytes 24580
  298.3 67.4 %copy-start.10 = (f32[8,2]{0,1:T(2,128)S(1)}, f32[8,2]{0,1:T(2,128)}, u32[]{:S(2)}) copy-start(f32[8,2]{0,1:T(2,128)} %param.42) | copy-start | bytes 196
  299.2 102.5 %copy-start.2 = (bf16[8,2048]{1,0:T(8,128)(2,1)S(1)}, bf16[8,2048]{1,0:T(8,128)(2,1)}, u32[]{:S(2)}) copy-start(bf16[8,2048]{1,0:T(8,128)(2,1)} %param.23) | copy-start | bytes 98308
  299.2 102.7 %copy-start.7 = (f32[2048]{0:T(1024)S(1)}, f32[2048]{0:T(1024)}, u32[]{:S(2)}) copy-start(f32[2048]{0:T(1024)} %param.36) | copy-start | bytes 24580
  299.2 59.0 %all-to-all-start.1 = ((bf16[128,8,256]{2,1,0:T(8,128)(2,1)}), bf16[128,8,256]{2,1,0:T(8,128)(2,1)S(1)}, u32[]{:S(2)}, u32[]{:S(2)}) async-start(bf16[128,8,256]{2,1,0:T(8,128)(2,1)} %stack.4), calls=%async_computation.2 | async-start | bytes 1048576 | tf_op jit(solution)/shard_map/all_to_all | solution.py:16
  359.3 28.8 %all-to-all-start.2 = ((bf16[128,8,16]{2,1,0:T(8,128)(2,1)}), bf16[128,8,16]{2,1,0:T(8,128)(2,1)S(1)}, u32[]{:S(2)}, u32[]{:S(2)}) async-start(bf16[128,8,16]{2,1,0:T(8,128)(2,1)} %bitcast.19), calls=%async_computation.3 | async-start | bytes 524288 | tf_op jit(solution)/shard_map/all_to_all | solution.py:38
  403.1 32.5 %all-to-all-start.3 = ((bf16[8,128,16]{2,0,1:T(8,128)(2,1)}), bf16[8,128,16]{2,0,1:T(8,128)(2,1)S(1)}, u32[]{:S(2)}, u32[]{:S(2)}) async-start(bf16[8,128,16]{2,0,1:T(8,128)(2,1)} %copy.108), calls=%async_computation.4 | async-start | bytes 524288 | tf_op jit(solution)/shard_map/all_to_all | solution.py:25
  413.4 30.2 %copy-start.4 = (bf16[16,256]{1,0:T(8,128)(2,1)S(1)}, bf16[16,256]{1,0:T(8,128)(2,1)}, u32[]{:S(2)}) copy-start(bf16[16,256]{1,0:T(8,128)(2,1)} %param.38) | copy-start | bytes 24580
  413.4 30.2 %copy-start.5 = (bf16[16,256]{1,0:T(8,128)(2,1)S(1)}, bf16[16,256]{1,0:T(8,128)(2,1)}, u32[]{:S(2)}) copy-start(bf16[16,256]{1,0:T(8,128)(2,1)} %param.37) | copy-start | bytes 24580
  437.3 262.7 %all-to-all-start.6 = ((bf16[128,2,2048]{2,1,0:T(2,128)(2,1)}), bf16[128,2,2048]{2,1,0:T(2,128)(2,1)S(1)}, u32[]{:S(2)}, u32[]{:S(2)}) async-start(bf16[128,2,2048]{2,1,0:T(2,128)(2,1)} %bitcast.26), calls=%async_computation.8 | async-start | bytes 2097152 | tf_op jit(solution)/shard_map/all_to_all | solution.py:131
  443.5 255.7 %reduce-scatter.5.cloned.1.call-start = ((), (), s32[]{:S(2)}) async-start(), calls=%async_computation.12 | async-start | bytes 2113536 | tf_op jit(solution)/shard_map/reduce_scatter | solution.py:26
  445.4 280.7 %copy-start.16 = (bf16[1,2048,176]{1,2,0:T(8,128)(2,1)S(1)}, bf16[1,2048,176]{1,2,0:T(8,128)(2,1)}, u32[]{:S(2)}) copy-start(bf16[1,2048,176]{1,2,0:T(8,128)(2,1)} %param.43) | copy-start | bytes 2162692
  700.9 58.9 %all-to-all-start.4 = ((bf16[128,8,256]{2,1,0:T(8,128)(2,1)}), bf16[128,8,256]{2,1,0:T(8,128)(2,1)S(1)}, u32[]{:S(2)}, u32[]{:S(2)}) async-start(bf16[128,8,256]{2,1,0:T(8,128)(2,1)} %stack.5), calls=%async_computation.6 | async-start | bytes 1048576 | tf_op jit(solution)/shard_map/all_to_all | solution.py:16
  732.1 31.6 %copy-start.6 = (bf16[256,16]{0,1:T(8,128)(2,1)S(1)}, bf16[256,16]{0,1:T(8,128)(2,1)}, u32[]{:S(2)}) copy-start(bf16[256,16]{0,1:T(8,128)(2,1)} %param.39) | copy-start | bytes 24580
  759.7 19.1 %all-to-all-start.7 = ((bf16[128,1,2,2048]{0,2,1,3:T(2,128)(2,1)}), bf16[128,1,2,2048]{0,2,1,3:T(2,128)(2,1)S(1)}, u32[]{:S(2)}, u32[]{:S(2)}) async-start(bf16[128,1,2,2048]{0,2,1,3:T(2,128)(2,1)} %copy.116), calls=%async_computation.9 | async-start | bytes 2097152 | tf_op jit(solution)/shard_map/all_to_all | solution.py:141
  778.8 28.9 %all-to-all-start.5 = ((bf16[128,8,16]{2,1,0:T(8,128)(2,1)}), bf16[128,8,16]{2,1,0:T(8,128)(2,1)S(1)}, u32[]{:S(2)}, u32[]{:S(2)}) async-start(bf16[128,8,16]{2,1,0:T(8,128)(2,1)} %bitcast.24), calls=%async_computation.7 | async-start | bytes 524288 | tf_op jit(solution)/shard_map/all_to_all | solution.py:38
  785.2 28.8 %copy-start.8 = (f32[2048]{0:T(1024)S(1)}, f32[2048]{0:T(1024)}, u32[]{:S(2)}) copy-start(f32[2048]{0:T(1024)} %param.40) | copy-start | bytes 24580
  807.8 28.8 %all-to-all-start.8 = ((bf16[128,1,2,512]{3,2,1,0:T(2,128)(2,1)}), bf16[128,1,2,512]{3,2,1,0:T(2,128)(2,1)S(1)}, u32[]{:S(2)}, u32[]{:S(2)}) async-start(bf16[128,1,2,512]{3,2,1,0:T(2,128)(2,1)} %copy.118), calls=%async_computation.10 | async-start | bytes 524288 | tf_op jit(solution)/shard_map/all_to_all | solution.py:146
Sparse Core Ops, SparseCore 0:
  53.0 242.0 reduce-scatter.2
  449.0 250.2 reduce-scatter.4
